TPU v7x, 32 devices: a whole 2x2x4 slice. The times are simulated.
32 devices in a mesh: fs: 8 (over z, x), tp: 4 (over y, core).
Axes of the slice: x: 2, y: 2, z: 4, core: 2. Of those that a mesh axis runs over, the one named last changes fastest.
Arguments:
- tokens: bfloat16 [2048, 2048], P('fs'), may hold values from -6 to 6
- norm_gain: float32 [2048], P('fs'), may hold values from 0.1 to 1.9
- gate_weight: float32 [8, 2048, 2048], P(None, 'fs', 'tp'), as said below
- up_weight: float32 [8, 2048, 2048], P(None, 'fs', 'tp'), as said below
- down_weight: float32 [8, 2048, 2048], P(None, 'fs', 'tp'), may hold values from -0.125 to 0.125
- routes: int32 [2048, 4], P('fs'), may hold values from 0 to 7, all different within a row; in each aligned block of 256 rows (0 to 255, 256 to 511, ...) at most 192 rows name the same one
- route_weights: bfloat16 [2048, 4], P('fs'), may hold values from 0.049804688 to 0.59765625
Outputs:
- gate_ready: bfloat16 [8, 2048, 2048], P('fs', None, 'tp')
- up_ready: bfloat16 [8, 2048, 2048], P('fs', None, 'tp')
- down_ready: bfloat16 [8, 2048, 2048], P('fs', None, 'tp')
- moe_output: bfloat16 [2048, 2048], P('fs', 'tp')
Inputs may be any that keep to these rules, and one draw needn't show every extreme that they name: `routes`: each row names 4 different experts; among the rows of one index of fs no expert is named more than 192 times. `gate_weight`: real-valued entries, drawn afresh for each expert; the scale may differ from column to column. `up_weight`: real-valued entries, drawn afresh for each expert; the scale may differ from column to column.
All inputs are finite; a program needn't handle non-finite values.
Results may differ from a plain program's by a relative error of at most 0.015.
Values may be sent and summed in bfloat16 or wider, within the bound.
A program may use at most 128 MiB of HBM per device.

v0:
```python
import jax
import jax.numpy as jnp
from jax import lax
from jax.sharding import PartitionSpec as P

norm_eps = 1e-06
clamp_limit = 7.0
gate_alpha = 1.702


def slot_numbers(route_block, capacity, experts):
    flat_routes = route_block.reshape(-1)
    onehot = (flat_routes[:, None] == jnp.arange(experts, dtype=jnp.int32)[None, :]).astype(
        jnp.int32
    )
    earlier = jnp.cumsum(onehot, axis=0) - onehot
    position = jnp.sum(earlier * onehot, axis=1)
    return flat_routes * capacity + position


def slot_sources(slots, top_count, tok_rows, total_slots):
    owners = jnp.arange(slots.shape[0], dtype=jnp.int32) // top_count
    return jnp.full((total_slots,), tok_rows, jnp.int32).at[slots].set(owners)


def combine_table(slots, weights_block, total_slots):
    matches = (
        slots.reshape(weights_block.shape)[:, :, None]
        == jnp.arange(total_slots, dtype=jnp.int32)[None, None, :]
    )
    table = jnp.sum(
        jnp.where(matches, weights_block.astype(jnp.float32)[:, :, None], jnp.float32(0.0)), axis=1
    )
    return table.astype(jnp.bfloat16)


def activate(gate_pre, up_pre):
    gate_part = jnp.minimum(gate_pre, clamp_limit)
    up_part = jnp.clip(up_pre, -clamp_limit, clamp_limit)
    return (up_part + 1.0) * gate_part * jax.nn.sigmoid(gate_alpha * gate_part)


def body(tokens, norm_gain, gate_weight, up_weight, down_weight, routes, route_weights):
    experts = lax.axis_size("fs")
    groups = lax.axis_size("tp")
    tok_rows = tokens.shape[0]
    top_count = routes.shape[1]
    model_width = tokens.shape[1]
    capacity = 3 * tok_rows * top_count // (2 * experts)
    total_slots = experts * capacity
    gain_col = norm_gain[None, :, None]
    gate_local = (gain_col * gate_weight).astype(jnp.bfloat16)
    up_local = (gain_col * up_weight).astype(jnp.bfloat16)
    down_local = down_weight.astype(jnp.bfloat16)
    gate_ready, up_ready, down_ready = (
        lax.all_to_all(gate_local, "fs", split_axis=0, concat_axis=1, tiled=True),
        lax.all_to_all(up_local, "fs", split_axis=0, concat_axis=1, tiled=True),
        lax.all_to_all(down_local, "fs", split_axis=0, concat_axis=1, tiled=True),
    )
    wide_tokens = tokens.astype(jnp.float32)
    normed = (
        wide_tokens
        * lax.rsqrt(jnp.mean(wide_tokens * wide_tokens, axis=1, keepdims=True) + norm_eps)
    ).astype(jnp.bfloat16)
    slots = slot_numbers(routes, capacity, experts)
    sources = slot_sources(slots, top_count, tok_rows, total_slots)
    padded = jnp.concatenate([normed, jnp.zeros((1, model_width), jnp.bfloat16)], axis=0)
    part_width = model_width // groups
    columns = lax.dynamic_slice_in_dim(padded, lax.axis_index("tp") * part_width, part_width, 1)
    sent = columns[sources].reshape(experts, capacity, part_width)
    arrived = lax.all_to_all(sent, "fs", split_axis=0, concat_axis=0, tiled=True)
    shard_piece = lax.all_gather(arrived, "tp", axis=2, tiled=True)
    piece_width = shard_piece.shape[2]
    flat_piece = shard_piece.reshape(total_slots, piece_width)
    gate_piece = gate_ready[0]
    up_piece = up_ready[0]
    gate_pre = jnp.dot(flat_piece, gate_piece, preferred_element_type=jnp.float32)
    up_pre = jnp.dot(flat_piece, up_piece, preferred_element_type=jnp.float32)
    hidden = activate(gate_pre, up_pre).astype(jnp.bfloat16)
    down_piece = down_ready[0]
    summed = lax.psum_scatter(
        lax.dot_general(
            down_piece, hidden, (((1,), (1,)), ((), ())), preferred_element_type=jnp.float32
        ).astype(jnp.bfloat16),
        "tp",
        scatter_dimension=0,
        tiled=True,
    )
    returned = lax.all_to_all(summed, "fs", split_axis=1, concat_axis=1, tiled=True)
    table = combine_table(slots, route_weights, total_slots)
    moe_output = lax.dot_general(
        table, returned, (((1,), (1,)), ((), ())), preferred_element_type=jnp.float32
    ).astype(jnp.bfloat16)
    return (gate_ready, up_ready, down_ready, moe_output)


def solution(mesh):
    in_specs = (
        P("fs", None),
        P("fs"),
        P(None, "fs", "tp"),
        P(None, "fs", "tp"),
        P(None, "fs", "tp"),
        P("fs", None),
        P("fs", None),
    )
    out_specs = (P("fs", None, "tp"), P("fs", None, "tp"), P("fs", None, "tp"), P("fs", "tp"))
    return jax.shard_map(body, mesh=mesh, in_specs=in_specs, out_specs=out_specs, check_vma=False)
```

profile of v0, /device:TPU:19, one launch (start us, length us, event | category | flops | bytes accessed | tf_op | source)
XLA Modules:
  0.0 348.6 jit_solution(13996113408955302982)
XLA Ops:
  7.2 0.9 copy.17
  8.4 2.3 reduce-window.6
  10.6 0.3 slice_reduce_fusion
  10.9 0.2 reduce-window.9
  11.2 0.1 reduce_sum.32
  11.3 0.1 mul.71
  11.5 4.3 %scatter_custom_fusion = s32[1536]{0:T(1024)S(1)} fusion(s32[1024]{0:T(1024)S(1)} %bitcast.45, s32[1024]{0:T(1024)S(1)} %add_select_fusion, s32[]{:T(128)} %constant.49.clone.1), kind=kCustom, calls=%fused_computation.40 | custom fusion | bytes 6148 | tf_op jit(solution)/shard_map/scatter | solution.py:23
  15.8 1.5 fusion.5
  17.4 0.2 fusion.6
  17.7 5.4 %gather_fusion = bf16[1536,512]{1,0:T(8,128)(2,1)} fusion(bf16[257,512]{1,0:T(8,128)(2,1)S(1)} %pad_dynamic-slice_fusion, s32[2048]{0:T(1024)S(1)} %pad_clamp_fusion), kind=kCustom, calls=%fused_computation | custom fusion | bytes 3151872 | tf_op jit(solution)/shard_map/gather | solution.py:70
  23.1 5.7 %all-to-all-start.3 = ((bf16[8,192,512]{2,1,0:T(8,128)(2,1)}), bf16[8,192,512]{2,1,0:T(8,128)(2,1)S(1)}, u32[]{:S(2)}, u32[]{:S(2)}) async-start(bf16[8,192,512]{2,1,0:T(8,128)(2,1)} %bitcast.6), calls=%async_computation.3 | async-start | bytes 3145728 | tf_op jit(solution)/shard_map/all_to_all | solution.py:71
  28.8 6.8 %multiply_convert_fusion = (bf16[8,256,512]{2,1,0:T(8,128)(2,1)}, bf16[8,256,512]{2,1,0:T(8,128)(2,1)}) fusion(f32[8,256,512]{2,1,0:T(8,128)} %param.10, f32[256]{0:T(256)S(1)} %copy-done.3, f32[8,256,512]{2,1,0:T(8,128)} %param.9), kind=kLoop, calls=%fused_computation.6 | loop fusion | flops 4194304 | bytes 12583936 | tf_op jit(solution)/shard_map/convert_element_type | solution.py:53
  35.6 26.7 %all-to-all-done.3 = bf16[8,192,512]{2,1,0:T(8,128)(2,1)S(1)} async-done(((bf16[8,192,512]{2,1,0:T(8,128)(2,1)}), bf16[8,192,512]{2,1,0:T(8,128)(2,1)S(1)}, u32[]{:S(2)}, u32[]{:S(2)}) %all-to-all-start.3) | async-done | bytes 1572896 | tf_op jit(solution)/shard_map/all_to_all | solution.py:71
  62.3 1.1 copy-done
  63.4 7.3 %all-to-all-start = ((bf16[8,256,512]{2,1,0:T(8,128)(2,1)}), bf16[8,256,512]{2,1,0:T(8,128)(2,1)S(1)}, u32[]{:S(2)}, u32[]{:S(2)}) async-start(bf16[8,256,512]{2,1,0:T(8,128)(2,1)} %get-tuple-element.7), calls=%async_computation | async-start | bytes 4194304 | tf_op jit(solution)/shard_map/all_to_all | solution.py:56
  70.7 0.7 all-gather.2.cloned.1.call-update
  71.4 44.1 %all-to-all-done = bf16[8,256,512]{2,1,0:T(8,128)(2,1)S(1)} async-done(((bf16[8,256,512]{2,1,0:T(8,128)(2,1)}), bf16[8,256,512]{2,1,0:T(8,128)(2,1)S(1)}, u32[]{:S(2)}, u32[]{:S(2)}) %all-to-all-start) | async-done | bytes 2097184 | tf_op jit(solution)/shard_map/all_to_all | solution.py:56
  115.5 7.3 %all-to-all-start.1 = ((bf16[8,256,512]{2,1,0:T(8,128)(2,1)}), bf16[8,256,512]{2,1,0:T(8,128)(2,1)}, u32[]{:S(2)}, u32[]{:S(2)}) async-start(bf16[8,256,512]{2,1,0:T(8,128)(2,1)} %get-tuple-element.6), calls=%async_computation.1 | async-start | bytes 4194304 | tf_op jit(solution)/shard_map/all_to_all | solution.py:57
  122.8 3.8 %convert_element_type.42 = bf16[8,256,512]{2,1,0:T(8,128)(2,1)} convert(f32[8,256,512]{2,1,0:T(8,128)} %param.11) | non-fusion elementwise | flops 1048576 | bytes 6291456 | tf_op jit(solution)/shard_map/convert_element_type | solution.py:54
  126.5 41.0 %all-to-all-done.1 = bf16[8,256,512]{2,1,0:T(8,128)(2,1)} async-done(((bf16[8,256,512]{2,1,0:T(8,128)(2,1)}), bf16[8,256,512]{2,1,0:T(8,128)(2,1)}, u32[]{:S(2)}, u32[]{:S(2)}) %all-to-all-start.1) | async-done | bytes 2097184 | tf_op jit(solution)/shard_map/all_to_all | solution.py:57
  167.6 7.4 %all-to-all-start.2 = ((bf16[8,256,512]{2,1,0:T(8,128)(2,1)}), bf16[8,256,512]{2,1,0:T(8,128)(2,1)}, u32[]{:S(2)}, u32[]{:S(2)}) async-start(bf16[8,256,512]{2,1,0:T(8,128)(2,1)} %convert_element_type.42), calls=%async_computation.2 | async-start | bytes 4194304 | tf_op jit(solution)/shard_map/all_to_all | solution.py:58
  174.9 7.9 %convolution_minimum_fusion = f32[1536,512]{1,0:T(8,128)} fusion(bf16[1536,2048]{1,0:T(8,128)(2,1)} %bitcast.46, bf16[2048,512]{1,0:T(8,128)(2,1)S(1)} %bitcast.40), kind=kOutput, calls=%fused_computation.9 | convolution fusion | flops 3222011904 | bytes 11534336 | tf_op jit(solution)/shard_map/dot_general | solution.py:77
  182.8 36.9 %all-to-all-done.2 = bf16[8,256,512]{2,1,0:T(8,128)(2,1)} async-done(((bf16[8,256,512]{2,1,0:T(8,128)(2,1)}), bf16[8,256,512]{2,1,0:T(8,128)(2,1)}, u32[]{:S(2)}, u32[]{:S(2)}) %all-to-all-start.2) | async-done | bytes 2097184 | tf_op jit(solution)/shard_map/all_to_all | solution.py:58
  219.7 12.4 %fusion = bf16[2048,1536]{0,1:T(8,128)(2,1)} fusion(bf16[2048,512]{1,0:T(8,128)(2,1)} %bitcast.10, f32[1536,512]{1,0:T(8,128)} %convolution_minimum_fusion, bf16[1536,2048]{1,0:T(8,128)(2,1)} %bitcast.47, bf16[2048,512]{1,0:T(8,128)(2,1)} %bitcast.8), kind=kOutput, calls=%fused_computation.3 | convolution fusion | flops 6452674560 | bytes 19922944 | tf_op jit(solution)/shard_map/dot_general | solution.py:82
  232.2 60.5 %reduce-scatter.2.cloned.1.call-done = bf16[512,1536]{0,1:T(8,128)(2,1)} async-done(((bf16[2048,1536]{0,1:T(8,128)(2,1)}), bf16[512,1536]{0,1:T(8,128)(2,1)}) %reduce-scatter.2.cloned.1.call-update) | async-done | bytes 1572880 | tf_op jit(solution)/shard_map/reduce_scatter | solution.py:81
  292.7 5.5 %all-to-all-start.4 = ((bf16[512,8,192]{0,2,1:T(8,128)(2,1)}), bf16[512,8,192]{0,2,1:T(8,128)(2,1)}, u32[]{:S(2)}, u32[]{:S(2)}) async-start(bf16[512,8,192]{0,2,1:T(8,128)(2,1)} %bitcast.42), calls=%async_computation.5 | async-start | bytes 3145728 | tf_op jit(solution)/shard_map/all_to_all | solution.py:89
  298.3 1.1 select_reduce_fusion
  299.4 32.3 %all-to-all-done.4 = bf16[512,8,192]{0,2,1:T(8,128)(2,1)} async-done(((bf16[512,8,192]{0,2,1:T(8,128)(2,1)}), bf16[512,8,192]{0,2,1:T(8,128)(2,1)}, u32[]{:S(2)}, u32[]{:S(2)}) %all-to-all-start.4) | async-done | bytes 1572896 | tf_op jit(solution)/shard_map/all_to_all | solution.py:89
  331.7 2.7 convolution_convert_fusion.1
  334.4 1.3 copy.26
  335.7 3.0 copy.27
  338.8 3.0 copy.28
  (25 shorter events, 0.5 us)
Async XLA Ops:
  7.2 10.2 %copy-start.1 = (bf16[256,2048]{1,0:T(8,128)(2,1)S(1)}, bf16[256,2048]{1,0:T(8,128)(2,1)}, u32[]{:S(2)}) copy-start(bf16[256,2048]{1,0:T(8,128)(2,1)} %param.7) | copy-start | bytes 3145732
  23.1 5.7 %copy-start.3 = (f32[256]{0:T(256)S(1)}, f32[256]{0:T(256)}, u32[]{:S(2)}) copy-start(f32[256]{0:T(256)} %param.8) | copy-start | bytes 3076
  23.1 39.2 %all-to-all-start.3 = ((bf16[8,192,512]{2,1,0:T(8,128)(2,1)}), bf16[8,192,512]{2,1,0:T(8,128)(2,1)S(1)}, u32[]{:S(2)}, u32[]{:S(2)}) async-start(bf16[8,192,512]{2,1,0:T(8,128)(2,1)} %bitcast.6), calls=%async_computation.3 | async-start | bytes 3145728 | tf_op jit(solution)/shard_map/all_to_all | solution.py:71
  62.3 1.1 copy-start
  63.4 52.1 %all-to-all-start = ((bf16[8,256,512]{2,1,0:T(8,128)(2,1)}), bf16[8,256,512]{2,1,0:T(8,128)(2,1)S(1)}, u32[]{:S(2)}, u32[]{:S(2)}) async-start(bf16[8,256,512]{2,1,0:T(8,128)(2,1)} %get-tuple-element.7), calls=%async_computation | async-start | bytes 4194304 | tf_op jit(solution)/shard_map/all_to_all | solution.py:56
  70.7 104.2 %all-gather.2.cloned.1.call-start = ((), (), s32[]{:S(2)}) async-start(), calls=%async_computation.6 | async-start | bytes 7864320 | tf_op jit(solution)/shard_map/all_gather | solution.py:72
  115.5 52.1 %all-to-all-start.1 = ((bf16[8,256,512]{2,1,0:T(8,128)(2,1)}), bf16[8,256,512]{2,1,0:T(8,128)(2,1)}, u32[]{:S(2)}, u32[]{:S(2)}) async-start(bf16[8,256,512]{2,1,0:T(8,128)(2,1)} %get-tuple-element.6), calls=%async_computation.1 | async-start | bytes 4194304 | tf_op jit(solution)/shard_map/all_to_all | solution.py:57
  167.6 52.2 %all-to-all-start.2 = ((bf16[8,256,512]{2,1,0:T(8,128)(2,1)}), bf16[8,256,512]{2,1,0:T(8,128)(2,1)}, u32[]{:S(2)}, u32[]{:S(2)}) async-start(bf16[8,256,512]{2,1,0:T(8,128)(2,1)} %convert_element_type.42), calls=%async_computation.2 | async-start | bytes 4194304 | tf_op jit(solution)/shard_map/all_to_all | solution.py:58
  174.9 117.8 %reduce-scatter.2.cloned.1.call-start = ((), (), s32[]{:S(2)}) async-start(), calls=%async_computation.7 | async-start | bytes 7864320 | tf_op jit(solution)/shard_map/reduce_scatter | solution.py:81
  232.2 66.1 %copy-start.2 = (bf16[256,4]{0,1:T(4,128)(2,1)S(1)}, bf16[256,4]{0,1:T(4,128)(2,1)}, u32[]{:S(2)}) copy-start(bf16[256,4]{0,1:T(4,128)(2,1)} %param.13) | copy-start | bytes 6148
  292.7 39.0 %all-to-all-start.4 = ((bf16[512,8,192]{0,2,1:T(8,128)(2,1)}), bf16[512,8,192]{0,2,1:T(8,128)(2,1)}, u32[]{:S(2)}, u32[]{:S(2)}) async-start(bf16[512,8,192]{0,2,1:T(8,128)(2,1)} %bitcast.42), calls=%async_computation.5 | async-start | bytes 3145728 | tf_op jit(solution)/shard_map/all_to_all | solution.py:89
Sparse Core Ops, SparseCore 0:
  73.6 48.0 all-gather.1
  232.3 60.3 reduce-scatter.1
where the time goes:
time: 355 us; the launch traced here: 349 us
  waiting for transfers between devices  242 us (68%)
  starting transfers between devices  33.1 us (9%)
  matrix products  23 us (6%)
  local copies, waits for them, and re-layouts  20.1 us (6%)
  other arithmetic  16 us (5%)
  between operations  14.2 us (4%)
    reduce_scatter x1, waiting for transfers between devices, body(): lax.psum_scatter(lax.dot_general(down_piece, hidden, (((1,), (1,)), ((),...  60.5 us
    all_to_all x1, waiting for transfers between devices, body(): lax.all_to_all(gate_local, 'fs', split_axis=0, concat_axis=1, tiled=True)  44.1 us
    all_to_all x1, waiting for transfers between devices, body(): lax.all_to_all(up_local, 'fs', split_axis=0, concat_axis=1, tiled=True)  41 us
    all_to_all x1, waiting for transfers between devices, body(): lax.all_to_all(down_local, 'fs', split_axis=0, concat_axis=1, tiled=True)  36.9 us
    all_to_all x1, waiting for transfers between devices, body(): lax.all_to_all(summed, 'fs', split_axis=1, concat_axis=1, tiled=True)  32.3 us
    all_to_all x1, waiting for transfers between devices, body(): lax.all_to_all(sent, 'fs', split_axis=0, concat_axis=0, tiled=True)  26.7 us
    dot_general x1, matrix products, body(): lax.dot_general(down_piece, hidden, (((1,), (1,)), ((), ())), preferred_e...  12.4 us
    unnamed x12, local copies, waits for them, and re-layouts  9.47 us
  transfers between devices with their start and end apart: 7, of which 6 were waited for; matrix products, arithmetic and copies ran while one was open for 6% of the time, Pallas kernels for 0%

commit v1 on v0

v1 whole, which is shorter than its diff:
```python
import functools

import jax
import jax.numpy as jnp
from jax import lax
from jax.experimental import pallas as pl
from jax.experimental.pallas import tpu as pltpu
from jax.sharding import PartitionSpec as P

norm_eps = 1e-06
clamp_limit = 7.0
gate_alpha = 1.702
MESH = pl.DeviceIdType.MESH
CORES = 2


def activate(gate_pre, up_pre):
    gate_part = jnp.minimum(gate_pre, clamp_limit)
    up_part = jnp.clip(up_pre, -clamp_limit, clamp_limit)
    return (up_part + 1.0) * gate_part * jax.nn.sigmoid(gate_alpha * gate_part)


def earlier_counts(member):
    rows = member.shape[1]
    before = (
        jnp.arange(rows, dtype=jnp.int32)[:, None] < jnp.arange(rows, dtype=jnp.int32)[None, :]
    ).astype(jnp.bfloat16)
    return jnp.dot(
        member.astype(jnp.bfloat16), before, preferred_element_type=jnp.float32
    ).astype(jnp.int32)


def kernel(
    n,
    groups,
    row_tile,
    sent,
    gate_local,
    up_local,
    down_local,
    gate_ready,
    up_ready,
    down_ready,
    returned,
    routed,
    hidden,
    kept,
    given,
    partner_sums,
    chip_sums,
    finished,
    dispatch_send,
    dispatch_recv,
    share_send,
    share_recv,
    weight_send,
    weight_recv,
    pair_send,
    pair_recv,
    chip_send,
    chip_recv,
    return_send,
    return_recv,
    own_sem,
):
    me = lax.axis_index("fs")
    tp = lax.axis_index("tp")
    chips = groups // CORES
    chip = tp // CORES
    core = lax.rem(tp, CORES)
    partner = chip * CORES + (CORES - 1 - core)
    capacity = sent.shape[0] // n
    source_rows = gate_local.shape[1]
    part = sent.shape[1]
    shares = n // groups
    total_slots = n * capacity

    def slots_of(block):
        return pl.ds(pl.multiple_of(block * capacity, 16), capacity)

    def rows_of(block):
        return pl.ds(pl.multiple_of(block * source_rows, 16), source_rows)

    barrier = pltpu.get_barrier_semaphore()
    for k in range(1, n):
        pl.semaphore_signal(
            barrier, inc=1, device_id=(lax.rem(me + k, n), tp), device_id_type=MESH
        )
    for k in range(1, groups):
        pl.semaphore_signal(
            barrier, inc=1, device_id=(me, lax.rem(tp + k, groups)), device_id_type=MESH
        )
    pl.semaphore_wait(barrier, n + groups - 2)

    waits = []

    dispatch = {}
    for k in range(1, n):
        peer = lax.rem(me + k, n)
        copy = pltpu.make_async_remote_copy(
            src_ref=sent.at[slots_of(peer)],
            dst_ref=routed.at[tp, slots_of(me)],
            send_sem=dispatch_send.at[k],
            recv_sem=dispatch_recv.at[k],
            device_id=(peer, tp),
            device_id_type=MESH,
        )
        copy.start()
        dispatch[k] = copy
    own_tokens = pltpu.make_async_copy(
        sent.at[slots_of(me)], routed.at[tp, slots_of(me)], own_sem.at[3]
    )
    own_tokens.start()
    own_weights = []
    weights = {}
    locals_ = (gate_local, up_local, down_local)
    readies = (gate_ready, up_ready, down_ready)
    for j in range(3):
        copy = pltpu.make_async_copy(locals_[j].at[me], readies[j].at[rows_of(me)], own_sem.at[j])
        copy.start()
        own_weights.append(copy)
    for turn in ((0, 1), (2,)):
        for k in range(1, n):
            peer = lax.rem(me + k, n)
            for j in turn:
                copy = pltpu.make_async_remote_copy(
                    src_ref=locals_[j].at[peer],
                    dst_ref=readies[j].at[rows_of(me)],
                    send_sem=weight_send.at[j, k],
                    recv_sem=weight_recv.at[j, k],
                    device_id=(peer, tp),
                    device_id_type=MESH,
                )
                copy.start()
                weights[j, k] = copy

    for k in range(n):
        source = lax.rem(me - k + n, n)
        if k == 0:
            own_tokens.wait()
        else:
            dispatch[k].wait_recv()
        for step in range(1, groups):
            pltpu.make_async_remote_copy(
                src_ref=routed.at[tp, slots_of(source)],
                dst_ref=routed.at[tp, slots_of(source)],
                send_sem=share_send.at[step],
                recv_sem=share_recv.at[step],
                device_id=(me, lax.rem(tp + step, groups)),
                device_id_type=MESH,
            ).start()
    share_waits = []
    for step in range(1, groups):
        origin = lax.rem(tp - step + groups, groups)
        share = pltpu.make_async_remote_copy(
            src_ref=routed.at[tp],
            dst_ref=routed.at[origin],
            send_sem=share_send.at[step],
            recv_sem=share_recv.at[step],
            device_id=(me, lax.rem(tp + step, groups)),
            device_id_type=MESH,
        )
        share.wait_recv()
        share_waits.append(share)

    for j in range(2):
        own_weights[j].wait()
        for k in range(1, n):
            weights[j, k].wait_recv()

    @pl.loop(0, total_slots // row_tile)
    def _(tile):
        rows = pl.ds(pl.multiple_of(tile * row_tile, 16), row_tile)
        gate_pre = jnp.zeros((row_tile, hidden.shape[1]), jnp.float32)
        up_pre = jnp.zeros((row_tile, hidden.shape[1]), jnp.float32)
        for t in range(groups):
            piece = routed[t, rows, :]
            gate_pre += jnp.dot(
                piece, gate_ready[t * part : (t + 1) * part], preferred_element_type=jnp.float32
            )
            up_pre += jnp.dot(
                piece, up_ready[t * part : (t + 1) * part], preferred_element_type=jnp.float32
            )
        hidden[rows, :] = activate(gate_pre, up_pre).astype(jnp.bfloat16)

    own_weights[2].wait()

    def arrival(source):
        k = lax.rem(me - source + n, n)

        @pl.when(k > 0)
        def _():
            pltpu.make_async_remote_copy(
                src_ref=down_local.at[0],
                dst_ref=down_ready.at[rows_of(source)],
                send_sem=weight_send.at[2, k],
                recv_sem=weight_recv.at[2, k],
                device_id=(me, partner),
                device_id_type=MESH,
            ).wait_recv()

    def project(source, out, slot):
        down = down_ready[rows_of(source), :]

        @pl.loop(0, total_slots // row_tile)
        def _(tile):
            rows = pl.ds(pl.multiple_of(tile * row_tile, 16), row_tile)
            out[slot, rows, :] = lax.dot_general(
                hidden[rows, :], down, (((1,), (1,)), ((), ())), preferred_element_type=jnp.float32
            ).astype(jnp.bfloat16)

    sums = []
    order = [(h, r) for h in range(1, chips) for r in range(shares)]
    order += [(0, r) for r in range(shares)]

    def start_group(h, r):
        slot = h * shares + r
        to_chip = lax.rem(chip + h, chips)
        give_source = (to_chip * CORES + (CORES - 1 - core)) * shares + r
        keep_source = (to_chip * CORES + core) * shares + r
        arrival(give_source)
        project(give_source, given, slot)
        pair = pltpu.make_async_remote_copy(
            src_ref=given.at[slot],
            dst_ref=partner_sums.at[slot],
            send_sem=pair_send.at[slot],
            recv_sem=pair_recv.at[slot],
            device_id=(me, partner),
            device_id_type=MESH,
        )
        pair.start()
        arrival(keep_source)
        project(keep_source, kept, slot)
        return pair

    for h, r in order:
        slot = h * shares + r
        pair = start_group(h, r)
        pair.wait_recv()
        waits.append(pair)
        if h > 0:

            @pl.loop(0, total_slots // row_tile)
            def _(tile):
                rows = pl.ds(pl.multiple_of(tile * row_tile, 16), row_tile)
                total = kept[slot, rows, :].astype(jnp.float32)
                total += partner_sums[slot, rows, :].astype(jnp.float32)
                kept[slot, rows, :] = total.astype(jnp.bfloat16)

            over = pltpu.make_async_remote_copy(
                src_ref=kept.at[slot],
                dst_ref=chip_sums.at[slot - shares],
                send_sem=chip_send.at[slot - shares],
                recv_sem=chip_recv.at[slot - shares],
                device_id=(me, lax.rem(chip + h, chips) * CORES + core),
                device_id_type=MESH,
            )
            over.start()
            sums.append((r, over))
            waits.append(over)
        else:
            for share, over in sums:
                if share == r:
                    over.wait_recv()

            @pl.loop(0, total_slots // row_tile)
            def _(tile):
                rows = pl.ds(pl.multiple_of(tile * row_tile, 16), row_tile)
                total = kept[slot, rows, :].astype(jnp.float32)
                total += partner_sums[slot, rows, :].astype(jnp.float32)
                for other in range(1, chips):
                    total += chip_sums[(other - 1) * shares + r, rows, :].astype(jnp.float32)
                finished[r, rows, :] = total.astype(jnp.bfloat16)

            for k in range(1, n):
                peer = lax.rem(me + k, n)
                back = pltpu.make_async_remote_copy(
                    src_ref=finished.at[r, slots_of(peer)],
                    dst_ref=returned.at[r, slots_of(me)],
                    send_sem=return_send.at[r, k],
                    recv_sem=return_recv.at[r, k],
                    device_id=(peer, tp),
                    device_id_type=MESH,
                )
                back.start()
                waits.append(back)
                sums.append((-1, back))
            own = pltpu.make_async_copy(
                finished.at[r, slots_of(me)], returned.at[r, slots_of(me)], own_sem.at[4 + r]
            )
            own.start()
            own_weights.append(own)

    for share, back in sums:
        if share == -1:
            back.wait_recv()
    for own in own_weights[3:]:
        own.wait()
    for copy in waits + share_waits + list(dispatch.values()) + list(weights.values()):
        copy.wait_send()


def hand_over(sent, gate_local, up_local, down_local):
    n = lax.axis_size("fs")
    groups = lax.axis_size("tp")
    total_slots, part = sent.shape
    source_rows, units = gate_local.shape[1:]
    width = n * source_rows
    shares = n // groups
    chips = groups // CORES
    vmem = pl.BlockSpec(memory_space=pltpu.VMEM)
    anywhere = pl.BlockSpec(memory_space=pl.ANY)
    bf16 = jnp.bfloat16
    ready = jax.ShapeDtypeStruct((width, units), bf16)
    dma = pltpu.SemaphoreType.DMA
    return pl.pallas_call(
        functools.partial(kernel, n, groups, total_slots // 4),
        out_shape=(
            ready,
            ready,
            ready,
            jax.ShapeDtypeStruct((shares, total_slots, source_rows), bf16),
        ),
        in_specs=[anywhere] * 4,
        out_specs=(vmem,) * 4,
        scratch_shapes=[
            pltpu.VMEM((groups, total_slots, part), bf16),
            pltpu.VMEM((total_slots, units), bf16),
            pltpu.VMEM((chips * shares, total_slots, source_rows), bf16),
            pltpu.VMEM((chips * shares, total_slots, source_rows), bf16),
            pltpu.VMEM((chips * shares, total_slots, source_rows), bf16),
            pltpu.VMEM(((chips - 1) * shares, total_slots, source_rows), bf16),
            pltpu.VMEM((shares, total_slots, source_rows), bf16),
            dma((n,)),
            dma((n,)),
            dma((groups,)),
            dma((groups,)),
            dma((3, n)),
            dma((3, n)),
            dma((chips * shares,)),
            dma((chips * shares,)),
            dma(((chips - 1) * shares,)),
            dma(((chips - 1) * shares,)),
            dma((shares, n)),
            dma((shares, n)),
            dma((4 + shares,)),
        ],
        compiler_params=pltpu.CompilerParams(
            collective_id=0, has_side_effects=True, vmem_limit_bytes=52 * 1024 * 1024
        ),
    )(sent, gate_local, up_local, down_local)


def body(tokens, norm_gain, gate_weight, up_weight, down_weight, routes, route_weights):
    experts = lax.axis_size("fs")
    groups = lax.axis_size("tp")
    tok_rows, model_width = tokens.shape
    top_count = routes.shape[1]
    capacity = 3 * tok_rows * top_count // (2 * experts)
    total_slots = experts * capacity
    part_width = model_width // groups

    gate_local = (norm_gain[None, :, None] * gate_weight).astype(jnp.bfloat16)
    up_local = (norm_gain[None, :, None] * up_weight).astype(jnp.bfloat16)
    down_local = down_weight.astype(jnp.bfloat16)

    wide_tokens = tokens.astype(jnp.float32)
    scale = lax.rsqrt(jnp.mean(wide_tokens * wide_tokens, axis=1, keepdims=True) + norm_eps)
    start = lax.axis_index("tp") * part_width
    columns = (
        lax.dynamic_slice_in_dim(tokens, start, part_width, 1).astype(jnp.float32) * scale
    ).astype(jnp.bfloat16)

    chosen = routes.T[:, None, :] == jnp.arange(experts, dtype=jnp.int32)[None, :, None]
    member = jnp.sum(chosen.astype(jnp.int32), axis=0)
    position = jnp.where(member > 0, earlier_counts(member), -1)
    row_weight = jnp.sum(
        jnp.where(chosen, route_weights.T.astype(jnp.float32)[:, None, :], 0.0), axis=0
    )
    here = position[:, None, :] == jnp.arange(capacity, dtype=jnp.int32)[None, :, None]
    pick = here.astype(jnp.bfloat16).reshape(total_slots, tok_rows)
    table = (
        jnp.where(here, row_weight[:, None, :], jnp.float32(0.0))
        .astype(jnp.bfloat16)
        .reshape(total_slots, tok_rows)
    )
    sent = jnp.dot(pick, columns, preferred_element_type=jnp.float32).astype(jnp.bfloat16)

    gate_ready, up_ready, down_ready, returned = hand_over(
        sent, gate_local, up_local, down_local
    )
    moe_output = jnp.concatenate(
        [
            lax.dot_general(
                table, piece, (((0,), (0,)), ((), ())), preferred_element_type=jnp.float32
            ).astype(jnp.bfloat16)
            for piece in returned
        ],
        axis=1,
    )
    return (gate_ready[None], up_ready[None], down_ready[None], moe_output)


def solution(mesh):
    in_specs = (
        P("fs", None),
        P("fs"),
        P(None, "fs", "tp"),
        P(None, "fs", "tp"),
        P(None, "fs", "tp"),
        P("fs", None),
        P("fs", None),
    )
    out_specs = (P("fs", None, "tp"), P("fs", None, "tp"), P("fs", None, "tp"), P("fs", "tp"))
    return jax.shard_map(body, mesh=mesh, in_specs=in_specs, out_specs=out_specs, check_vma=False)
```

time: 355 us -> 255 us (0.72); the launches traced: 349 us -> 255 us
  waiting for transfers between devices: 242 us -> 0 us
  Pallas kernels: 0 us -> 232 us
  starting transfers between devices: 33.1 us -> 0 us
  matrix products: 23 us -> 3.76 us
  between operations: 14.2 us -> 0.73 us
  local copies, waits for them, and re-layouts: 20.1 us -> 7.23 us
  other arithmetic: 16 us -> 11.3 us
    pallas_call x0 -> x1, Pallas kernels: none -> 232 us  [hand_over(): pl.pallas_call(functools.partial(kernel, n, groups, total_slots // 4), ou...]
    all_to_all x5 -> x0, waiting for transfers between devices: 181 us -> none  [the longest x1 44.1 us: body(): lax.all_to_all(gate_local, 'fs', split_axis=0, concat_axis=1, tiled=True)]
    reduce_scatter x1 -> x0, waiting for transfers between devices: 60.5 us -> none  [body(): lax.psum_scatter(lax.dot_general(down_piece, hidden, (((1,), (1,)), ((),...]
    all_to_all x5 -> x0, starting transfers between devices: 33.1 us -> none  [the longest x1 7.36 us: body(): lax.all_to_all(down_local, 'fs', split_axis=0, concat_axis=1, tiled=True)]
    dot_general x3 -> x4, matrix products: 23 us -> 3.76 us  [the longest x1 2.76 us: body(): jnp.dot(pick, columns, preferred_element_type=jnp.float32)]
    gather x1 -> x0, local copies, waits for them, and re-layouts: 5.41 us -> none  [body(): sent = columns[sources].reshape(experts, capacity, part_width)]
    scatter x1 -> x0, local copies, waits for them, and re-layouts: 4.32 us -> none  [slot_sources(): return jnp.full((total_slots,), tok_rows, jnp.int32).at[slots].set(owners)]
    unnamed x12 -> x18, local copies, waits for them, and re-layouts: 9.47 us -> 7.15 us
  transfers between devices with their start and end apart: 7 -> 0, of which waited for: 6 -> 0; matrix products, arithmetic and copies ran while one was open for 6% -> 0% of each run, Pallas kernels for 0% -> 0%
where the time goes in v1:
time: 255 us
  Pallas kernels  232 us (91%)
  other arithmetic  11.3 us (4%)
  local copies, waits for them, and re-layouts  7.23 us (3%)
  matrix products  3.76 us (1%)
    pallas_call x1, Pallas kernels, hand_over(): pl.pallas_call(functools.partial(kernel, n, groups, total_slots // 4), ou...  232 us
    unnamed x18, local copies, waits for them, and re-layouts  7.15 us
    convert_element_type x1, other arithmetic, body(): up_local = (norm_gain[None, :, None] * up_weight).astype(jnp.bfloat16)  6.95 us

profile of v1, /device:TPU:19, one launch (start us, length us, event | category | flops | bytes accessed | tf_op | source)
XLA Modules:
  0.0 255.0 jit_solution(15525427986113434902)
XLA Ops:
  0.6 0.0 copy-start.6
  0.6 0.7 convert_reduce_fusion
  1.3 0.2 fusion
  1.5 0.1 eq.55
  1.6 0.3 bitcast_compare_fusion
  1.9 1.5 multiply_reduce_fusion
  3.4 2.8 %convolution_convert_fusion.sent = bf16[1536,512]{1,0:T(8,128)(2,1)} fusion(pred[1536,256]{1,0:T(32,128)(4,1)S(1)} %bitcast_compare_fusion, f32[256]{0:T(256)S(1)} %add_rsqrt_fusion, bf16[256,2048]{1,0:T(8,128)(2,1)} %param.7, s32[]{:T(128)S(6)} %select_n.28), kind=kOutput, calls=%fused_computation.2 | convolution fusion | flops 403832832 | bytes 2229252 | tf_op jit(solution)/shard_map/dot_general | solution.py:387
  6.1 0.0 copy-done.6
  6.2 0.0 copy-start
  6.2 7.0 %multiply_convert_fusion = (bf16[8,256,512]{2,1,0:T(8,128)(2,1)}, bf16[8,256,512]{2,1,0:T(8,128)(2,1)}) fusion(f32[8,256,512]{2,1,0:T(8,128)} %param.10, f32[256]{0:T(256)S(1)} %copy-done.6, f32[8,256,512]{2,1,0:T(8,128)} %param.9), kind=kLoop, calls=%fused_computation | loop fusion | flops 4194304 | bytes 12583936 | tf_op jit(solution)/shard_map/convert_element_type | solution.py:364
  13.1 0.0 copy-done
  13.1 1.6 convert_element_type.70.down_local
  14.7 0.0 copy-start.5
  14.7 0.0 copy-start.4
  14.7 232.0 %shard_map.102 = (bf16[2048,512]{1,0:T(8,128)(2,1)}, bf16[2048,512]{1,0:T(8,128)(2,1)}, bf16[2048,512]{1,0:T(8,128)(2,1)}, bf16[2,1536,256]{2,1,0:T(8,128)(2,1)S(1)}) custom-call(bf16[1536,512]{1,0:T(8,128)(2,1)} %convolution_convert_fusion.sent, bf16[8,256,512]{2,1,0:T(8,128)(2,1)} %get-tuple-element.21.gate_local, ...), custom_call_target="tpu_custom_call" | custom-call | tf_op jit(solution)/shard_map/pallas_call | solution.py:316
  246.7 0.0 copy-done.5
  246.7 0.0 copy-done.4
  246.7 0.2 select_convert_fusion
  247.0 0.4 convolution_convert_fusion.1
  247.4 0.0 copy-start.3
  247.4 0.4 convolution_convert_fusion.2
  247.9 0.8 copy.12
  248.7 0.3 copy-done.3
  249.0 0.0 copy-start.2
  249.0 1.3 copy.18
  250.3 1.0 copy-done.2
  251.4 0.0 copy-start.1
  251.4 1.3 copy.19
  252.7 1.0 copy-done.1
  253.7 1.3 copy.20
  (5 shorter events, 0.0 us)
Async XLA Ops:
  0.6 5.5 %copy-start.6 = (f32[256]{0:T(256)S(1)}, f32[256]{0:T(256)}, u32[]{:S(2)}) copy-start(f32[256]{0:T(256)} %param.8) | copy-start | bytes 3076
  6.2 7.0 %copy-start = (f32[8,256,512]{2,1,0:T(8,128)S(1)}, f32[8,256,512]{2,1,0:T(8,128)}, u32[]{:S(2)}) copy-start(f32[8,256,512]{2,1,0:T(8,128)} %param.11) | copy-start | bytes 12582916
  14.7 232.0 %copy-start.5 = (bf16[256,4]{0,1:T(4,128)(2,1)S(1)}, bf16[256,4]{0,1:T(4,128)(2,1)}, u32[]{:S(2)}) copy-start(bf16[256,4]{0,1:T(4,128)(2,1)} %param.13) | copy-start | bytes 6148
  14.7 232.0 %copy-start.4 = (s32[256,4]{0,1:T(4,128)S(1)}, s32[256,4]{0,1:T(4,128)}, u32[]{:S(2)}) copy-start(s32[256,4]{0,1:T(4,128)} %param.12) | copy-start | bytes 12292
  247.4 1.6 copy-start.3
  249.0 2.3 copy-start.2
  251.4 2.3 copy-start.1

commit v2 on v1

--- a/solution.py
+++ b/solution.py
@@ -12,6 +12,7 @@
 gate_alpha = 1.702
 MESH = pl.DeviceIdType.MESH
 CORES = 2
+DEPTH = 4
 
 
 def activate(gate_pre, up_pre):
@@ -35,6 +36,7 @@
     groups,
     row_tile,
     sent,
+    gain,
     gate_local,
     up_local,
     down_local,
@@ -49,6 +51,8 @@
     partner_sums,
     chip_sums,
     finished,
+    wide,
+    staged,
     dispatch_send,
     dispatch_recv,
     share_send,
@@ -62,6 +66,7 @@
     return_send,
     return_recv,
     own_sem,
+    wide_sem,
 ):
     me = lax.axis_index("fs")
     tp = lax.axis_index("tp")
@@ -81,6 +86,20 @@
     def rows_of(block):
         return pl.ds(pl.multiple_of(block * source_rows, 16), source_rows)
 
+    locals_ = (gate_local, up_local, down_local)
+    readies = (gate_ready, up_ready, down_ready)
+    blocks = [(j, k) for turn in ((0, 1), (2,)) for k in range(n) for j in turn]
+
+    def fetch(i):
+        j, k = blocks[i]
+        copy = pltpu.make_async_copy(
+            locals_[j].at[lax.rem(me + k, n)], wide.at[i % DEPTH], wide_sem.at[i % DEPTH]
+        )
+        copy.start()
+        return copy
+
+    fetches = [fetch(i) for i in range(DEPTH)]
+
     barrier = pltpu.get_barrier_semaphore()
     for k in range(1, n):
         pl.semaphore_signal(
@@ -108,31 +127,38 @@
         copy.start()
         dispatch[k] = copy
     own_tokens = pltpu.make_async_copy(
-        sent.at[slots_of(me)], routed.at[tp, slots_of(me)], own_sem.at[3]
+        sent.at[slots_of(me)], routed.at[tp, slots_of(me)], own_sem.at[0]
     )
     own_tokens.start()
-    own_weights = []
+    own_copies = []
     weights = {}
-    locals_ = (gate_local, up_local, down_local)
-    readies = (gate_ready, up_ready, down_ready)
-    for j in range(3):
-        copy = pltpu.make_async_copy(locals_[j].at[me], readies[j].at[rows_of(me)], own_sem.at[j])
+
+    def send(j, k):
+        copy = pltpu.make_async_remote_copy(
+            src_ref=staged.at[j, k - 1],
+            dst_ref=readies[j].at[rows_of(me)],
+            send_sem=weight_send.at[j, k],
+            recv_sem=weight_recv.at[j, k],
+            device_id=(lax.rem(me + k, n), tp),
+            device_id_type=MESH,
+        )
         copy.start()
-        own_weights.append(copy)
-    for turn in ((0, 1), (2,)):
-        for k in range(1, n):
-            peer = lax.rem(me + k, n)
-            for j in turn:
-                copy = pltpu.make_async_remote_copy(
-                    src_ref=locals_[j].at[peer],
-                    dst_ref=readies[j].at[rows_of(me)],
-                    send_sem=weight_send.at[j, k],
-                    recv_sem=weight_recv.at[j, k],
-                    device_id=(peer, tp),
-                    device_id_type=MESH,
-                )
-                copy.start()
-                weights[j, k] = copy
+        weights[j, k] = copy
+
+    for i, (j, k) in enumerate(blocks):
+        fetches[i].wait()
+        value = wide[i % DEPTH]
+        if j < 2:
+            value = gain[...] * value
+        if k == 0:
+            readies[j][rows_of(me), :] = value.astype(jnp.bfloat16)
+        else:
+            staged[j, k - 1] = value.astype(jnp.bfloat16)
+        if i + DEPTH < len(blocks):
+            fetches.append(fetch(i + DEPTH))
+        if i > 0 and blocks[i - 1][1] > 0:
+            send(*blocks[i - 1])
+    send(*blocks[-1])
 
     for k in range(n):
         source = lax.rem(me - k + n, n)
@@ -164,7 +190,6 @@
         share_waits.append(share)
 
     for j in range(2):
-        own_weights[j].wait()
         for k in range(1, n):
             weights[j, k].wait_recv()
 
@@ -183,15 +208,13 @@
             )
         hidden[rows, :] = activate(gate_pre, up_pre).astype(jnp.bfloat16)
 
-    own_weights[2].wait()
-
     def arrival(source):
         k = lax.rem(me - source + n, n)
 
         @pl.when(k > 0)
         def _():
             pltpu.make_async_remote_copy(
-                src_ref=down_local.at[0],
+                src_ref=staged.at[2, 0],
                 dst_ref=down_ready.at[rows_of(source)],
                 send_sem=weight_send.at[2, k],
                 recv_sem=weight_recv.at[2, k],
@@ -286,21 +309,21 @@
                 waits.append(back)
                 sums.append((-1, back))
             own = pltpu.make_async_copy(
-                finished.at[r, slots_of(me)], returned.at[r, slots_of(me)], own_sem.at[4 + r]
+                finished.at[r, slots_of(me)], returned.at[r, slots_of(me)], own_sem.at[1 + r]
             )
             own.start()
-            own_weights.append(own)
+            own_copies.append(own)
 
     for share, back in sums:
         if share == -1:
             back.wait_recv()
-    for own in own_weights[3:]:
+    for own in own_copies:
         own.wait()
     for copy in waits + share_waits + list(dispatch.values()) + list(weights.values()):
         copy.wait_send()
 
 
-def hand_over(sent, gate_local, up_local, down_local):
+def hand_over(sent, gain, gate_local, up_local, down_local):
     n = lax.axis_size("fs")
     groups = lax.axis_size("tp")
     total_slots, part = sent.shape
@@ -321,7 +344,7 @@
             ready,
             jax.ShapeDtypeStruct((shares, total_slots, source_rows), bf16),
         ),
-        in_specs=[anywhere] * 4,
+        in_specs=[anywhere, vmem] + [anywhere] * 3,
         out_specs=(vmem,) * 4,
         scratch_shapes=[
             pltpu.VMEM((groups, total_slots, part), bf16),
@@ -331,6 +354,8 @@
             pltpu.VMEM((chips * shares, total_slots, source_rows), bf16),
             pltpu.VMEM(((chips - 1) * shares, total_slots, source_rows), bf16),
             pltpu.VMEM((shares, total_slots, source_rows), bf16),
+            pltpu.VMEM((DEPTH, source_rows, units), jnp.float32),
+            pltpu.VMEM((3, n - 1, source_rows, units), bf16),
             dma((n,)),
             dma((n,)),
             dma((groups,)),
@@ -343,12 +368,13 @@
             dma(((chips - 1) * shares,)),
             dma((shares, n)),
             dma((shares, n)),
-            dma((4 + shares,)),
+            dma((1 + shares,)),
+            dma((DEPTH,)),
         ],
         compiler_params=pltpu.CompilerParams(
             collective_id=0, has_side_effects=True, vmem_limit_bytes=52 * 1024 * 1024
         ),
-    )(sent, gate_local, up_local, down_local)
+    )(sent, gain, gate_local, up_local, down_local)
 
 
 def body(tokens, norm_gain, gate_weight, up_weight, down_weight, routes, route_weights):
@@ -360,10 +386,6 @@
     total_slots = experts * capacity
     part_width = model_width // groups
 
-    gate_local = (norm_gain[None, :, None] * gate_weight).astype(jnp.bfloat16)
-    up_local = (norm_gain[None, :, None] * up_weight).astype(jnp.bfloat16)
-    down_local = down_weight.astype(jnp.bfloat16)
-
     wide_tokens = tokens.astype(jnp.float32)
     scale = lax.rsqrt(jnp.mean(wide_tokens * wide_tokens, axis=1, keepdims=True) + norm_eps)
     start = lax.axis_index("tp") * part_width
@@ -387,7 +409,7 @@
     sent = jnp.dot(pick, columns, preferred_element_type=jnp.float32).astype(jnp.bfloat16)
 
     gate_ready, up_ready, down_ready, returned = hand_over(
-        sent, gate_local, up_local, down_local
+        sent, norm_gain[:, None], gate_weight, up_weight, down_weight
     )
     moe_output = jnp.concatenate(
         [

time: 255 us -> 247 us (0.969)
  other arithmetic: 11.3 us -> 2.78 us
    convert_element_type x2 -> x0, other arithmetic: 8.54 us -> none  [the longest x1 6.95 us: body(): up_local = (norm_gain[None, :, None] * up_weight).astype(jnp.bfloat16)]
    unnamed x18 -> x16, local copies, waits for them, and re-layouts: 7.15 us -> 7.15 us
where the time goes in v2:
time: 247 us
  Pallas kernels  232 us (94%)
  local copies, waits for them, and re-layouts  7.37 us (3%)
  matrix products  3.77 us (2%)
  other arithmetic  2.78 us (1%)
    pallas_call x1, Pallas kernels, hand_over(): pl.pallas_call(functools.partial(kernel, n, groups, total_slots // 4), ou...  232 us
    unnamed x16, local copies, waits for them, and re-layouts  7.15 us

profile of v2, /device:TPU:19, one launch (start us, length us, event | category | flops | bytes accessed | tf_op | source)
XLA Modules:
  0.0 246.8 jit_solution(8188723395024510664)
XLA Ops:
  0.6 0.0 copy-start.5
  0.6 0.7 convert_reduce_fusion
  1.3 0.2 fusion
  1.5 0.1 eq.55
  1.6 0.3 bitcast_compare_fusion
  1.9 1.5 multiply_reduce_fusion
  3.4 2.8 %convolution_convert_fusion.sent = bf16[1536,512]{1,0:T(8,128)(2,1)} fusion(pred[1536,256]{1,0:T(32,128)(4,1)S(1)} %bitcast_compare_fusion, f32[256]{0:T(256)S(1)} %add_rsqrt_fusion, bf16[256,2048]{1,0:T(8,128)(2,1)} %param.7, s32[]{:T(128)S(6)} %select_n.28), kind=kOutput, calls=%fused_computation | convolution fusion | flops 403832832 | bytes 2229252 | tf_op jit(solution)/shard_map/dot_general | solution.py:409
  6.2 0.0 copy-done.5
  6.2 0.1 copy.14.gain
  6.3 0.0 copy-start.4
  6.3 0.0 copy-start.3
  6.3 232.1 %shard_map.102 = (bf16[2048,512]{1,0:T(8,128)(2,1)}, bf16[2048,512]{1,0:T(8,128)(2,1)}, bf16[2048,512]{1,0:T(8,128)(2,1)}, bf16[2,1536,256]{2,1,0:T(8,128)(2,1)S(1)}) custom-call(bf16[1536,512]{1,0:T(8,128)(2,1)} %convolution_convert_fusion.sent, f32[256,1]{1,0:T(8,128)S(1)} %copy.14.gain, f32[8,256,512]{2,1,0:T(8,128)} %gate_local.1, ...), custom_call_target="tpu_custom_call" | custom-call | tf_op jit(solution)/shard_map/pallas_call | solution.py:339
  238.4 0.0 copy-done.4
  238.4 0.0 copy-done.3
  238.5 0.2 select_convert_fusion
  238.7 0.4 convolution_convert_fusion.1
  239.1 0.0 copy-start.2
  239.2 0.4 convolution_convert_fusion.2
  239.6 0.8 copy.15
  240.5 0.3 copy-done.2
  240.7 0.0 copy-start.1
  240.7 1.3 copy.21
  242.1 1.0 copy-done.1
  243.1 0.0 copy-start
  243.1 1.3 copy.22
  244.4 1.0 copy-done
  245.4 1.3 copy.23
  (5 shorter events, 0.0 us)
Async XLA Ops:
  0.6 5.5 %copy-start.5 = (f32[256]{0:T(256)S(1)}, f32[256]{0:T(256)}, u32[]{:S(2)}) copy-start(f32[256]{0:T(256)} %param.8) | copy-start | bytes 3076
  6.3 232.1 %copy-start.4 = (bf16[256,4]{0,1:T(4,128)(2,1)S(1)}, bf16[256,4]{0,1:T(4,128)(2,1)}, u32[]{:S(2)}) copy-start(bf16[256,4]{0,1:T(4,128)(2,1)} %param.13) | copy-start | bytes 6148
  6.3 232.1 %copy-start.3 = (s32[256,4]{0,1:T(4,128)S(1)}, s32[256,4]{0,1:T(4,128)}, u32[]{:S(2)}) copy-start(s32[256,4]{0,1:T(4,128)} %param.12) | copy-start | bytes 12292
  239.1 1.6 copy-start.2
  240.7 2.3 copy-start.1
  243.1 2.3 copy-start
